TPU v7x, 32 devices: a whole 2x2x4 slice. The times are simulated.
32 devices in a mesh: sp: 4 (over x, core), dp: 8 (over z, y).
Axes of the slice: x: 2, y: 2, z: 4, core: 2. Of those that a mesh axis runs over, the one named last changes fastest.
Arguments:
- content_features_raw: bfloat16 [8, 512, 3072], P('dp', 'sp'), may hold values from -6 to 6
- memory_entering_matrix: bfloat16 [8, 512, 2048], P('dp', 'sp'), may hold values from -6 to 6
- memory_leaving_matrix: bfloat16 [8, 512, 2048], P('dp', 'sp'), may hold values from -6 to 6
- feature_switch_signal: bfloat16 [8, 512, 3072], P('dp', 'sp'), may hold values from -6 to 6
- ahead_increment_raw: float32 [8, 512, 48], P('dp', 'sp'), may hold values from -5 to 5
- reverse_increment_raw: float32 [8, 512, 48], P('dp', 'sp'), may hold values from -5 to 5
- additional_fading: float32 [8, 512, 48], P('dp', 'sp'), as said below
- content_filter_weights: bfloat16 [4, 3072], P(None, 'sp'), may hold values from -3 to 3
- entering_filter_weights: bfloat16 [4, 2048], P(None, 'sp'), may hold values from -3 to 3
- leaving_filter_weights: bfloat16 [4, 2048], P(None, 'sp'), may hold values from -3 to 3
- increment_offset_lanes: float32 [2, 48], P(None, 'sp'), may hold values from -0.5 to 0.5
- fading_speed_exponents: float32 [2, 48], P(None, 'sp'), as said below
- result_scaling_factor: bfloat16 [3072], replicated, may hold values from 0.099609375 to 1.8984375
Outputs:
- out: bfloat16 [8, 512, 3072], P('dp', 'sp')
Inputs may be any that keep to these rules, and one draw needn't show every extreme that they name: Each head's row has a rate exp(fading_speed_exponents) between 0.3 / 4096 and 0.05. `additional_fading`: zero at most positions; elsewhere between log(0.5) and log(0.8).
All inputs are finite; a program needn't handle non-finite values.
Results may differ from a plain program's by a relative error of at most 0.0051.
Values may be sent and summed in bfloat16 or wider, within the bound.
A program may use at most 64 MiB of HBM per device.

v0:
```python
import functools

import jax
import jax.numpy as jnp
from jax import lax
from jax.experimental import pallas as pl
from jax.experimental.pallas import tpu as pltpu
from jax.sharding import PartitionSpec as P

F32 = jnp.float32
BF16 = jnp.bfloat16
HEAD_DIM = 64
STATE = 128
HIGHEST = lax.Precision.HIGHEST


def levels_of(sp, dp, groups):
    found = []
    split = 1
    core = 2 if sp % 2 == 0 else 1
    inner = 2 if dp % 2 == 0 and groups % (2 * sp) == 0 else 1
    for axis, count, stride in (("sp", core, 1), ("sp", sp // core, core), ("dp", inner, 1)):
        if count > 1:
            found.append((axis, count, stride))
            split *= count
    return tuple(found), ("dp", dp // inner, inner)


def digit_of(level):
    axis, count, stride = level
    return lax.rem(lax.axis_index(axis) // stride, count)


def member_id(level, member):
    axis, count, stride = level
    return {axis: lax.axis_index(axis) + (member - digit_of(level)) * stride}


def kernel(levels, top, sizes, *refs):
    heads, pairs = sizes
    (x_ref, b_ref, c_ref, z_ref, inc_ref, spike_ref, prm_ref, w_ref, halo_ref, gain_ref) = refs[:10]
    out_ref = refs[10]
    (xc, bc, cc, y_ref, cum_ref, rate_ref, cum_t, rate_t, fac_ref, first_total, first_log) = refs[11:22]
    rest = list(refs[22:])
    up, up_log, down, stage, totals, logs, sems = [], [], [], [], [first_total], [first_log], []
    for _ in levels:
        up.append(rest.pop(0))
        up_log.append(rest.pop(0))
        down.append(rest.pop(0))
        stage.append(rest.pop(0))
        totals.append(rest.pop(0))
        logs.append(rest.pop(0))
        sems.append(rest.pop(0))
    top_in, top_log, top_sem, incoming, decay = rest
    blk = x_ref.shape[0]
    per_pair = heads // pairs
    x_w = per_pair * HEAD_DIM
    b_w = 2 * STATE
    tiles = x_w // 128
    lane = lax.broadcasted_iota(jnp.int32, (blk, 128), 1)
    left = lane < HEAD_DIM
    row = lax.broadcasted_iota(jnp.int32, (blk, 128), 0)

    barrier = pltpu.get_barrier_semaphore()
    greeted = 0
    for level in levels + (top,):
        me = digit_of(level)
        for o in range(1, level[1]):
            pl.semaphore_signal(
                barrier,
                inc=1,
                device_id=member_id(level, lax.rem(me + o, level[1])),
                device_id_type=pl.DeviceIdType.MESH,
            )
            greeted += 1

    rate = jax.nn.softplus(inc_ref[...] + prm_ref[0:1, :])
    log_decay = -jnp.exp(prm_ref[1:2, :]) * rate + spike_ref[...]
    lower = (lane <= row).astype(F32)
    upper = (lane >= row).astype(F32)
    cum_f = jnp.dot(lower, log_decay, precision=HIGHEST, preferred_element_type=F32)
    cum_b = jnp.dot(upper, log_decay, precision=HIGHEST, preferred_element_type=F32)
    cum = jnp.where(lane < heads, cum_f, cum_b)
    lane1 = lane[0:1]
    last = jnp.where(lane1 < heads, cum_f[blk - 1 : blk], cum_b[0:1])
    cum_ref[...] = cum
    rate_ref[...] = rate
    cum_t[...] = cum.T
    rate_t[...] = rate.T
    fac_ref[...] = rate * jnp.exp(last - cum)
    first_log[...] = jnp.broadcast_to(last, (8, 128))

    def rolled(ref, p):
        return pltpu.roll(ref[...], lax.rem(128 - p * per_pair, 128), 1)

    def two(cols, i):
        return jnp.where(left, cols[:, i : i + 1], cols[:, i + 1 : i + 2])

    def conv(src, col, width, off):
        at = pl.ds(pl.multiple_of(off + col, 128), width)
        v = src[:, pl.ds(pl.multiple_of(col, 128), width)].astype(F32)
        r = lax.broadcasted_iota(jnp.int32, (blk, width), 0)
        h0, h1, h2 = halo_ref[0:1, at], halo_ref[1:2, at], halo_ref[2:3, at]
        m1 = jnp.where(r == 0, h1, pltpu.roll(v, 1, 0))
        m2 = jnp.where(r == 0, h0, jnp.where(r == 1, h1, pltpu.roll(v, 2, 0)))
        p1 = jnp.where(r == blk - 1, h2, pltpu.roll(v, blk - 1, 0))
        s = m2 * w_ref[0:1, at] + m1 * w_ref[1:2, at] + v * w_ref[2:3, at] + p1 * w_ref[3:4, at]
        return (s / (1.0 + jnp.exp(-s))).astype(BF16)

    x_total = x_ref.shape[1]
    b_total = b_ref.shape[1]

    def first(p, _):
        x_at = pl.ds(pl.multiple_of(p * x_w, 128), x_w)
        b_at = pl.ds(pl.multiple_of(p * b_w, 128), b_w)
        xv = conv(x_ref, p * x_w, x_w, 0)
        bv = conv(b_ref, p * b_w, b_w, x_total)
        xc[:, x_at] = xv
        bc[:, b_at] = bv
        cc[:, b_at] = conv(c_ref, p * b_w, b_w, x_total + b_total)
        cols = rolled(fac_ref, p)
        xf = xv.astype(F32)
        for d in range(2):
            scaled = jnp.concatenate(
                [
                    (xf[:, k * 128 : (k + 1) * 128] * two(cols, d * heads + 2 * k)).astype(BF16)
                    for k in range(tiles)
                ],
                axis=1,
            )
            u = lax.dot_general(scaled, bv, (((0,), (0,)), ((), ())), preferred_element_type=F32)
            half = x_w // 2
            rows = pl.ds(pl.multiple_of(p * x_w, 128), x_w)
            first_total[d, rows, :] = jnp.concatenate(
                [u[:half, :STATE], u[half:, STATE:]], axis=0
            ).astype(BF16)
        return 0

    lax.fori_loop(0, pairs, first, 0)
    pl.semaphore_wait(barrier, greeted)

    def inner(p, _):
        x_at = pl.ds(pl.multiple_of(p * x_w, 128), x_w)
        b_at = pl.ds(pl.multiple_of(p * b_w, 128), b_w)
        bv, cv, xv = bc[:, b_at], cc[:, b_at], xc[:, x_at]
        cols = rolled(cum_ref, p)
        parts = []
        for g in range(2):
            scores = lax.dot_general(
                cv[:, g * STATE : (g + 1) * STATE],
                bv[:, g * STATE : (g + 1) * STATE],
                (((1,), (1,)), ((), ())),
                preferred_element_type=F32,
            )
            for i in range(per_pair // 2):
                h = g * (per_pair // 2) + i
                hf = p * per_pair + h
                gap_f = cols[:, h : h + 1] - cum_t[pl.ds(hf, 1), :]
                gap_b = cols[:, heads + h : heads + h + 1] - cum_t[pl.ds(heads + hf, 1), :]
                gap = jnp.where(lane < row, gap_f, jnp.where(lane > row, gap_b, 0.0))
                rf, rb = rate_t[pl.ds(hf, 1), :], rate_t[pl.ds(heads + hf, 1), :]
                scale = jnp.where(lane < row, rf, jnp.where(lane > row, rb, rf + rb))
                parts.append((scores * jnp.exp(gap) * scale).astype(BF16))
        for k in range(tiles):
            xt = xv[:, k * 128 : (k + 1) * 128]
            zero = jnp.zeros_like(xt)
            both = jnp.concatenate([jnp.where(left, xt, zero), jnp.where(left, zero, xt)], axis=0)
            w = jnp.concatenate([parts[2 * k], parts[2 * k + 1]], axis=1)
            y_ref[:, pl.ds(pl.multiple_of(p * x_w + k * 128, 128), 128)] = jnp.dot(
                w, both, preferred_element_type=F32
            )
        return 0

    def copy(src, dst, send, recv, level, member):
        return pltpu.make_async_remote_copy(
            src_ref=src,
            dst_ref=dst,
            send_sem=send,
            recv_sem=recv,
            device_id=member_id(level, member),
            device_id_type=pl.DeviceIdType.MESH,
        )

    def expand(slot, tile):
        decay[slot] = jnp.exp(jnp.broadcast_to(tile[0:1, :], (128, 128)).T)

    slots = len(levels) + 1
    cuts = [(i * pairs) // slots for i in range(slots + 1)]
    base = jnp.int32(0)
    bases = []
    for k, level in enumerate(levels):
        n = level[1]
        me = digit_of(level)
        total, log = totals[k], logs[k]
        rows = total.shape[1] // n
        sem = sems[k]
        pending = []
        for o in range(1, n):
            m = lax.rem(me + o, n)
            part = total.at[:, pl.ds(pl.multiple_of(m * rows, 64), rows), :]
            pending.append(copy(part, up[k].at[me], sem.at[0, m], sem.at[1, me], level, m))
            pending.append(copy(log, up_log[k].at[me], sem.at[2, m], sem.at[3, me], level, m))
        for one in pending:
            one.start()
        up[k][me] = total[:, pl.ds(pl.multiple_of(me * rows, 64), rows), :]
        up_log[k][me] = log[...]
        lax.fori_loop(cuts[k], cuts[k + 1], inner, 0)
        for one in pending:
            one.wait_send()
        for o in range(1, n):
            s = lax.rem(me + o, n)
            part = total.at[:, pl.ds(0, rows), :]
            copy(part, up[k].at[s], sem.at[0, s], sem.at[1, s], level, s).wait_recv()
            copy(log, up_log[k].at[s], sem.at[2, s], sem.at[3, s], level, s).wait_recv()
        base = base + me * (rows // HEAD_DIM)
        bases.append(base)
        log_sum = up_log[k][0]
        for m in range(1, n):
            log_sum = log_sum + up_log[k][m]
        logs[k + 1][...] = log_sum
        for m in range(n):
            expand(m, up_log[k][m])

        def gather(h, _, k=k, n=n, base=base):
            at = pl.ds(pl.multiple_of(h * HEAD_DIM, HEAD_DIM), HEAD_DIM)
            f = up[k][0, 0, at, :].astype(F32)
            b = up[k][n - 1, 1, at, :].astype(F32)
            for m in range(1, n):
                f = f * decay[m, pl.ds(base + h, 1), :] + up[k][m, 0, at, :].astype(F32)
                r = n - 1 - m
                b = b * decay[r, pl.ds(heads + base + h, 1), :] + up[k][r, 1, at, :].astype(F32)
            totals[k + 1][0, at, :] = f.astype(BF16)
            totals[k + 1][1, at, :] = b.astype(BF16)
            return 0

        lax.fori_loop(0, rows // HEAD_DIM, gather, 0)

    n = top[1]
    me = digit_of(top)
    total, log = totals[-1], logs[-1]
    pending = []
    for o in range(1, n):
        m = lax.rem(me + o, n)
        d = jnp.where(m < me, 1, 0)
        pending.append(
            copy(total.at[d], top_in.at[me], top_sem.at[0, m], top_sem.at[1, me], top, m)
        )
        pending.append(copy(log, top_log.at[me], top_sem.at[2, m], top_sem.at[3, me], top, m))
    for one in pending:
        one.start()
    lax.fori_loop(cuts[-2], cuts[-1], inner, 0)
    for one in pending:
        one.wait_send()
    for o in range(1, n):
        s = lax.rem(me + o, n)
        copy(total.at[0], top_in.at[s], top_sem.at[0, s], top_sem.at[1, s], top, s).wait_recv()
        copy(log, top_log.at[s], top_sem.at[2, s], top_sem.at[3, s], top, s).wait_recv()
    incoming[...] = jnp.zeros_like(incoming)

    def carry(s, d):
        expand(0, top_log[s])

        def one_head(h, _):
            at = pl.ds(pl.multiple_of(h * HEAD_DIM, HEAD_DIM), HEAD_DIM)
            factor = decay[0, pl.ds(d * heads + base + h, 1), :]
            incoming[d, at, :] = incoming[d, at, :] * factor + top_in[s, at, :].astype(F32)
            return 0

        lax.fori_loop(0, total.shape[1] // HEAD_DIM, one_head, 0)
        return 0

    lax.fori_loop(0, me, lambda s, _: carry(s, 0), 0)
    lax.fori_loop(0, n - 1 - me, lambda i, _: carry(n - 1 - i, 1), 0)

    for k in reversed(range(len(levels))):
        level = levels[k]
        n = level[1]
        me = digit_of(level)
        sem = sems[k]
        rows = totals[k].shape[1] // n
        source = incoming if k == len(levels) - 1 else down[k + 1]
        for m in range(n):
            expand(m, up_log[k][m])

        def spread(h, _, k=k, n=n, base=bases[k], source=source):
            at = pl.ds(pl.multiple_of(h * HEAD_DIM, HEAD_DIM), HEAD_DIM)
            f = source[0, at, :].astype(F32)
            b = source[1, at, :].astype(F32)
            for m in range(n):
                r = n - 1 - m
                stage[k][m, 0, at, :] = f.astype(BF16)
                stage[k][r, 1, at, :] = b.astype(BF16)
                if m < n - 1:
                    f = f * decay[m, pl.ds(base + h, 1), :] + up[k][m, 0, at, :].astype(F32)
                    b = b * decay[r, pl.ds(heads + base + h, 1), :] + up[k][r, 1, at, :].astype(F32)
            return 0

        lax.fori_loop(0, rows // HEAD_DIM, spread, 0)
        mine = pl.ds(pl.multiple_of(me * rows, 64), rows)
        pending = []
        for o in range(1, n):
            m = lax.rem(me + o, n)
            pending.append(
                copy(stage[k].at[m], down[k].at[:, mine, :], sem.at[4, m], sem.at[5, me], level, m)
            )
        for one in pending:
            one.start()
        down[k][:, mine, :] = stage[k][me]
        for one in pending:
            one.wait_send()
        for o in range(1, n):
            s = lax.rem(me + o, n)
            theirs = pl.ds(pl.multiple_of(s * rows, 64), rows)
            copy(
                stage[k].at[s], down[k].at[:, theirs, :], sem.at[4, s], sem.at[5, s], level, s
            ).wait_recv()

    final = down[0] if levels else incoming
    cum_ref[...] = jnp.exp(cum_ref[...])

    def last_part(p, _):
        x_at = pl.ds(pl.multiple_of(p * x_w, 128), x_w)
        cv = cc[:, pl.ds(pl.multiple_of(p * b_w, 128), b_w)]
        cols = rolled(cum_ref, p)
        carried = []
        for d in range(2):
            st = final[d, x_at, :].astype(BF16)
            got = [
                lax.dot_general(
                    cv[:, g * STATE : (g + 1) * STATE],
                    st,
                    (((1,), (1,)), ((), ())),
                    preferred_element_type=F32,
                )
                for g in range(2)
            ]
            carried.append(got)
        for k in range(tiles):
            cut = slice(k * 128, (k + 1) * 128)
            at = pl.ds(pl.multiple_of(p * x_w + k * 128, 128), 128)
            y = y_ref[:, at]
            for d in range(2):
                a, b = carried[d][0][:, cut], carried[d][1][:, cut]
                if 2 * k + 1 < per_pair // 2:
                    v = a
                elif 2 * k >= per_pair // 2:
                    v = b
                else:
                    v = jnp.where(left, a, b)
                y = y + v * two(cols, d * heads + 2 * k)
            z = z_ref[:, at].astype(F32)
            gated = y.astype(BF16).astype(F32) * (z / (1.0 + jnp.exp(-z)))
            square = gated * gated
            low = jnp.sum(jnp.where(left, square, 0.0), axis=1, keepdims=True)
            high = jnp.sum(jnp.where(left, 0.0, square), axis=1, keepdims=True)
            mean = jnp.where(left, low, high) * (1.0 / HEAD_DIM)
            out_ref[:, at] = (gated * lax.rsqrt(mean + 1e-6) * gain_ref[0:1, at]).astype(BF16)
        return 0

    lax.fori_loop(0, pairs, last_part, 0)


def local(sp, dp, x, b, c, z, ahead, back, spike, wx, wb, wc, offset, fading, gain):
    x, b, c, z = x[0], b[0], c[0], z[0]
    blk, x_total = x.shape
    groups = b.shape[1] // STATE
    heads = ahead.shape[2]
    pairs = groups // 2
    xw, bw, hw = wx.shape[1], wb.shape[1], offset.shape[1]
    taps = jnp.concatenate([wx, wb, wc], axis=1).astype(F32)
    small = jnp.concatenate([offset, fading], axis=0)
    packed = jnp.concatenate([taps, jnp.pad(small, ((0, 0), (0, taps.shape[1] - hw)))], axis=0)
    every = lax.all_gather(packed, "sp")
    whole = jnp.transpose(every, (1, 0, 2))
    w = jnp.concatenate(
        [
            whole[:, :, :xw].reshape(8, -1),
            whole[:, :, xw : xw + bw].reshape(8, -1),
            whole[:, :, xw + bw :].reshape(8, -1),
        ],
        axis=1,
    )
    tail = jnp.zeros((128 - 2 * heads,), F32)
    flat = whole[4:8, :, :hw].reshape(4, heads)
    prm = jnp.stack(
        [jnp.concatenate([flat[0], flat[1], tail]), jnp.concatenate([flat[2], flat[3], tail])]
    )
    prm = jnp.pad(prm, ((0, 6), (0, 0)))
    count = sp * dp
    place = [(i % sp) * dp + i // sp for i in range(count)]
    ring = list(zip(place[:-1], place[1:]))
    edge = jnp.concatenate([x[-2:], b[-2:], c[-2:]], axis=1)
    head = jnp.concatenate([x[:1], b[:1], c[:1]], axis=1)
    before = lax.ppermute(edge, ("sp", "dp"), ring)
    after = lax.ppermute(head, ("sp", "dp"), [(j, i) for i, j in ring])
    halo = jnp.pad(jnp.concatenate([before, after], axis=0).astype(F32), ((0, 5), (0, 0)))
    pad = jnp.zeros((blk, 128 - 2 * heads), F32)
    inc = jnp.concatenate([ahead[0], back[0], pad], axis=1)
    spikes = jnp.concatenate([spike[0], spike[0], pad], axis=1)

    levels, top = levels_of(sp, dp, groups)
    scratch = [
        pltpu.VMEM((blk, x_total), BF16),
        pltpu.VMEM((blk, groups * STATE), BF16),
        pltpu.VMEM((blk, groups * STATE), BF16),
        pltpu.VMEM((blk, x_total), F32),
    ]
    scratch += [pltpu.VMEM((128, 128), F32)] * 5
    rows = x_total
    scratch += [pltpu.VMEM((2, rows, STATE), BF16), pltpu.VMEM((8, 128), F32)]
    widest = 1
    for _, n, _ in levels:
        widest = max(widest, n)
        scratch += [
            pltpu.VMEM((n, 2, rows // n, STATE), BF16),
            pltpu.VMEM((n, 8, 128), F32),
            pltpu.VMEM((2, rows, STATE), BF16),
            pltpu.VMEM((n, 2, rows // n, STATE), BF16),
            pltpu.VMEM((2, rows // n, STATE), BF16),
            pltpu.VMEM((8, 128), F32),
            pltpu.SemaphoreType.DMA((6, n)),
        ]
        rows //= n
    scratch += [
        pltpu.VMEM((top[1], rows, STATE), BF16),
        pltpu.VMEM((top[1], 8, 128), F32),
        pltpu.SemaphoreType.DMA((4, top[1])),
        pltpu.VMEM((2, rows, STATE), F32),
        pltpu.VMEM((widest, 128, 128), F32),
    ]
    out = pl.pallas_call(
        functools.partial(kernel, levels, top, (heads, pairs)),
        out_shape=jax.ShapeDtypeStruct((blk, x_total), BF16),
        in_specs=[pl.BlockSpec(memory_space=pltpu.VMEM)] * 10,
        out_specs=pl.BlockSpec(memory_space=pltpu.VMEM),
        scratch_shapes=scratch,
        compiler_params=pltpu.CompilerParams(
            collective_id=0, has_side_effects=True, vmem_limit_bytes=60 * 2**20
        ),
        name="mixer",
    )(x, b, c, z, inc, spikes, prm, w, halo, gain.astype(F32)[None])
    return out[None]


def solution(mesh):
    tokens = P("dp", "sp", None)
    placed = (tokens,) * 7 + (P(None, "sp"),) * 5 + (P(),)
    return jax.shard_map(
        functools.partial(local, mesh.shape["sp"], mesh.shape["dp"]),
        mesh=mesh,
        in_specs=placed,
        out_specs=tokens,
        check_vma=False,
    )
```

profile of v0, /device:TPU:9, one launch (start us, length us, event | category | flops | bytes accessed | tf_op | source)
XLA Modules:
  0.0 87.9 jit_solution(4259239766594351995)
XLA Ops:
  0.0 0.8 slice_bitcast_fusion.4
  0.8 0.8 slice_bitcast_fusion.7
  1.7 3.7 %collective-permute-start = (bf16[2,7168]{1,0:T(2,128)(2,1)S(1)}, bf16[2,7168]{1,0:T(2,128)(2,1)S(1)}, u32[]{:S(2)}, u32[]{:S(2)}) collective-permute-start(bf16[2,7168]{1,0:T(2,128)(2,1)S(1)} %pad_maximum_fusion.2), channel_id=1, source_target_pairs={{0,8},{8,16},{16,24},{24,1},{1,9},{9,17},{17,25},{25,2},{2,10},{10... | collective-permute-start | bytes 86024 | tf_op jit(solution)/shard_map/ppermute | solution.py:394
  5.3 0.8 slice_bitcast_fusion.3
  6.2 0.8 slice_bitcast_fusion.5
  6.9 0.0 copy-start.7
  7.0 0.0 copy-start.8
  7.0 0.0 copy-start.4
  7.0 0.0 copy-start.5
  7.0 0.0 copy-start.6
  7.1 2.1 %collective-permute-start.1 = (bf16[1,7168]{1,0:T(2,128)(2,1)S(1)}, bf16[1,7168]{1,0:T(2,128)(2,1)S(1)}, u32[]{:S(2)}, u32[]{:S(2)}) collective-permute-start(bf16[1,7168]{1,0:T(2,128)(2,1)S(1)} %pad_maximum_fusion.3), channel_id=1, source_target_pairs={{8,0},{16,8},{24,16},{1,24},{9,1},{17,9},{25,17},{2,25},{10,2},{18... | collective-permute-start | bytes 43016 | tf_op jit(solution)/shard_map/ppermute | solution.py:395
  9.1 0.0 copy-done.7
  9.1 0.0 copy-done.8
  9.1 0.0 copy-done.4
  9.2 0.0 copy-done.5
  9.2 0.0 copy-done.6
  9.2 8.0 %all-gather = f32[32,1792]{1,0:T(8,128)S(1)} all-gather(f32[8,1792]{1,0:T(8,128)S(1)} %pad_maximum_fusion.1), channel_id=2, replica_groups=mesh['sp'=4,'dp'=8] {'sp'}, dimensions={0}, use_global_device_ids=true | all-gather | bytes 286720 | tf_op jit(solution)/shard_map/all_gather | solution.py:373
  17.2 0.1 copy.22
  17.3 0.0 copy-start
  17.3 0.7 copy-done
  18.0 0.0 copy-start.1
  18.0 0.1 copy.14
  18.1 0.6 copy-done.1
  18.8 0.0 copy-start.2
  18.8 0.1 copy.15
  18.9 0.6 copy-done.2
  19.5 0.1 copy.16
  19.6 0.1 squeeze.41
  19.7 0.1 squeeze.44
  19.8 0.1 squeeze.43
  19.9 0.1 squeeze.42
  20.0 0.7 pad_maximum_fusion.refs_7_
  20.7 0.1 maximum_bitcast_fusion
  20.8 0.8 maximum_maximum_fusion.1
  21.6 0.0 copy-start.3
  21.6 0.6 select_maximum_fusion.1.refs_6_
  22.2 0.1 copy-done.3
  22.3 0.6 broadcast_in_dim.19
  22.9 0.0 collective-permute-done.1
  22.9 0.0 collective-permute-done
  22.9 0.8 fusion.3.refs_8_
  23.7 62.2 %mixer.1 = bf16[128,3072]{1,0:T(8,128)(2,1)} custom-call(bf16[128,3072]{1,0:T(8,128)(2,1)} %bitcast.43, bf16[128,2048]{1,0:T(8,128)(2,1)} %bitcast.45, bf16[128,2048]{1,0:T(8,128)(2,1)} %bitcast.46, bf16[128,3072]{1,0:T(8,128)(2,1)} %bitcast.44, f32[128,128]{1,0:T(8,128)} %get-tuple-element.15.refs_4_, f32[128,128]{1,0:T(8,128)} %get-tuple-element.14.refs_5_, ...), custom_call_target="tpu_custom_call" | custom-call | tf_op jit(solution)/shard_map/mixer/pallas_call | solution.py:431
  85.9 2.1 %copy.24 = bf16[1,128,3072]{2,1,0:T(8,128)(2,1)} copy(bf16[1,128,3072]{2,1,0:T(8,128)(2,1)} %bitcast.38) | data formatting | bytes 1572864
  (12 shorter events, 0.2 us)
Async XLA Ops:
  1.7 21.2 %collective-permute-start = (bf16[2,7168]{1,0:T(2,128)(2,1)S(1)}, bf16[2,7168]{1,0:T(2,128)(2,1)S(1)}, u32[]{:S(2)}, u32[]{:S(2)}) collective-permute-start(bf16[2,7168]{1,0:T(2,128)(2,1)S(1)} %pad_maximum_fusion.2), channel_id=1, source_target_pairs={{0,8},{8,16},{16,24},{24,1},{1,9},{9,17},{17,25},{25,2},{2,10},{10... | collective-permute-start | bytes 86024 | tf_op jit(solution)/shard_map/ppermute | solution.py:394
  6.9 2.2 %copy-start.7 = (f32[2,12]{1,0:T(2,128)S(1)}, f32[2,12]{1,0:T(2,128)}, u32[]{:S(2)}) copy-start(f32[2,12]{1,0:T(2,128)} %param.24) | copy-start | bytes 292
  7.0 2.2 %copy-start.8 = (f32[2,12]{1,0:T(2,128)S(1)}, f32[2,12]{1,0:T(2,128)}, u32[]{:S(2)}) copy-start(f32[2,12]{1,0:T(2,128)} %param.23) | copy-start | bytes 292
  7.0 2.1 %copy-start.4 = (bf16[4,768]{1,0:T(4,128)(2,1)S(1)}, bf16[4,768]{1,0:T(4,128)(2,1)}, u32[]{:S(2)}) copy-start(bf16[4,768]{1,0:T(4,128)(2,1)} %param.20) | copy-start | bytes 18436
  7.0 2.1 %copy-start.5 = (bf16[4,512]{1,0:T(4,128)(2,1)S(1)}, bf16[4,512]{1,0:T(4,128)(2,1)}, u32[]{:S(2)}) copy-start(bf16[4,512]{1,0:T(4,128)(2,1)} %param.22) | copy-start | bytes 12292
  7.0 2.1 %copy-start.6 = (bf16[4,512]{1,0:T(4,128)(2,1)S(1)}, bf16[4,512]{1,0:T(4,128)(2,1)}, u32[]{:S(2)}) copy-start(bf16[4,512]{1,0:T(4,128)(2,1)} %param.21) | copy-start | bytes 12292
  7.1 15.8 %collective-permute-start.1 = (bf16[1,7168]{1,0:T(2,128)(2,1)S(1)}, bf16[1,7168]{1,0:T(2,128)(2,1)S(1)}, u32[]{:S(2)}, u32[]{:S(2)}) collective-permute-start(bf16[1,7168]{1,0:T(2,128)(2,1)S(1)} %pad_maximum_fusion.3), channel_id=1, source_target_pairs={{8,0},{16,8},{24,16},{1,24},{9,1},{17,9},{25,17},{2,25},{10,2},{18... | collective-permute-start | bytes 43016 | tf_op jit(solution)/shard_map/ppermute | solution.py:395
  17.3 0.7 copy-start
  18.0 0.7 copy-start.1
  18.8 0.7 copy-start.2
  21.6 0.7 copy-start.3
where the time goes:
time: 88.6 us; the launch traced here: 87.9 us
  Pallas kernels  62.2 us (70%)
  local copies, waits for them, and re-layouts  8.2 us (9%)
  blocking collectives  7.96 us (9%)
  starting transfers between devices  5.73 us (6%)
  other arithmetic  3.61 us (4%)
    pallas_call x1, Pallas kernels, local(): pl.pallas_call(functools.partial(kernel, levels, top, (heads, pairs)), ou...  62.2 us
    all_gather x1, blocking collectives, local(): every = lax.all_gather(packed, 'sp')  7.96 us
    unnamed x27, local copies, waits for them, and re-layouts  4.56 us
    ppermute x1, starting transfers between devices, local(): before = lax.ppermute(edge, ('sp', 'dp'), ring)  3.68 us
    ppermute x1, starting transfers between devices, local(): after = lax.ppermute(head, ('sp', 'dp'), [(j, i) for i, j in ring])  2.05 us
  transfers between devices with their start and end apart: 2, of which 0 were waited for; matrix products, arithmetic and copies ran while one was open for 6% of the time, Pallas kernels for 0%

commit v1 on v0

--- a/solution.py
+++ b/solution.py
@@ -11,6 +11,7 @@
 BF16 = jnp.bfloat16
 HEAD_DIM = 64
 STATE = 128
+EDGE = 8
 HIGHEST = lax.Precision.HIGHEST
 
 
@@ -37,11 +38,15 @@
 
 
 def kernel(levels, top, sizes, *refs):
-    heads, pairs = sizes
-    (x_ref, b_ref, c_ref, z_ref, inc_ref, spike_ref, prm_ref, w_ref, halo_ref, gain_ref) = refs[:10]
-    out_ref = refs[10]
-    (xc, bc, cc, y_ref, cum_ref, rate_ref, cum_t, rate_t, fac_ref, first_total, first_log) = refs[11:22]
-    rest = list(refs[22:])
+    heads, pairs, sp, dp = sizes
+    (x_ref, b_ref, c_ref, z_ref, ahead_ref, back_ref, spike_ref) = refs[:7]
+    params = refs[7:12]
+    gain_ref, out_ref = refs[12:14]
+    (xc, bc, cc, y_ref, cum_ref, rate_ref, cum_t, rate_t, fac_ref, first_total, first_log) = refs[14:25]
+    got, w_ref, prm_ref, halo_ref, edges, early_sem, edge_sem = (
+        refs[25:30], refs[30], refs[31], refs[32], refs[33:39], refs[39], refs[40]
+    )
+    rest = list(refs[41:])
     up, up_log, down, stage, totals, logs, sems = [], [], [], [], [first_total], [first_log], []
     for _ in levels:
         up.append(rest.pop(0))
@@ -61,21 +66,89 @@
     left = lane < HEAD_DIM
     row = lax.broadcasted_iota(jnp.int32, (blk, 128), 0)
 
+    segment = ("sp", sp, 1)
+    here, there = lax.axis_index("sp"), lax.axis_index("dp")
+    rank = there * sp + here
+    has_next, has_prev = rank < sp * dp - 1, rank > 0
+    after = {"sp": lax.rem(here + 1, sp), "dp": lax.rem(there + (here + 1) // sp, dp)}
+    before = {
+        "sp": lax.rem(here + sp - 1, sp),
+        "dp": lax.rem(there + dp - (sp - here) // sp, dp),
+    }
+    mesh_id = pl.DeviceIdType.MESH
     barrier = pltpu.get_barrier_semaphore()
     greeted = 0
-    for level in levels + (top,):
+    for level in levels + (top, segment):
         me = digit_of(level)
         for o in range(1, level[1]):
-            pl.semaphore_signal(
-                barrier,
-                inc=1,
-                device_id=member_id(level, lax.rem(me + o, level[1])),
-                device_id_type=pl.DeviceIdType.MESH,
-            )
+            target = member_id(level, lax.rem(me + o, level[1]))
+            pl.semaphore_signal(barrier, inc=1, device_id=target, device_id_type=mesh_id)
             greeted += 1
-
-    rate = jax.nn.softplus(inc_ref[...] + prm_ref[0:1, :])
-    log_decay = -jnp.exp(prm_ref[1:2, :]) * rate + spike_ref[...]
+    for present, target in ((has_next, after), (has_prev, before)):
+
+        @pl.when(present)
+        def _(target=target):
+            pl.semaphore_signal(barrier, inc=1, device_id=target, device_id_type=mesh_id)
+
+    filler = jnp.zeros((128 - 2 * heads, blk), F32)
+    inc = jnp.concatenate([ahead_ref[...], back_ref[...], filler], axis=0).T
+    spikes = jnp.concatenate([spike_ref[...], spike_ref[...], filler], axis=0).T
+    count = sp * dp
+    neighbours = (rank + count - 1) // count + (2 * count - 2 - rank) // count
+    pl.semaphore_wait(barrier, greeted + neighbours)
+
+    def edge_copy(i, direction):
+        src = (x_ref, b_ref, c_ref)[i]
+        start = blk - EDGE if direction == 0 else 0
+        return pltpu.make_async_remote_copy(
+            src_ref=src.at[pl.ds(start, EDGE), :],
+            dst_ref=edges[3 * direction + i],
+            send_sem=edge_sem.at[0, direction, i],
+            recv_sem=edge_sem.at[1, direction, i],
+            device_id=(after, before)[direction],
+            device_id_type=mesh_id,
+        )
+
+    def param_copy(i, member, slot):
+        return pltpu.make_async_remote_copy(
+            src_ref=params[i],
+            dst_ref=got[i].at[slot],
+            send_sem=early_sem.at[0, i, member],
+            recv_sem=early_sem.at[1, i, slot],
+            device_id=member_id(segment, member),
+            device_id_type=mesh_id,
+        )
+
+    for o in range(1, sp):
+        for i in range(5):
+            param_copy(i, lax.rem(here + o, sp), here).start()
+    for direction, present in ((0, has_next), (1, has_prev)):
+
+        @pl.when(present)
+        def _(direction=direction):
+            for i in range(3):
+                edge_copy(i, direction).start()
+
+    for i in range(5):
+        got[i][here] = params[i][...]
+    for o in range(1, sp):
+        for i in range(5):
+            s = lax.rem(here + o, sp)
+            param_copy(i, s, s).wait_recv()
+    prm_ref[...] = jnp.zeros_like(prm_ref)
+    wide = got[3].shape[2]
+    for q in range(sp):
+        for kind in range(2):
+            for d in range(2):
+                at = slice(d * heads + q * wide, d * heads + (q + 1) * wide)
+                prm_ref[kind : kind + 1, at] = got[3 + kind][q, d : d + 1, :]
+        off = 0
+        for i in range(3):
+            n = got[i].shape[2]
+            w_ref[0:4, off + q * n : off + (q + 1) * n] = got[i][q].astype(F32)
+            off += n * sp
+    rate = jax.nn.softplus(inc + prm_ref[0:1, :])
+    log_decay = -jnp.exp(prm_ref[1:2, :]) * rate + spikes
     lower = (lane <= row).astype(F32)
     upper = (lane >= row).astype(F32)
     cum_f = jnp.dot(lower, log_decay, precision=HIGHEST, preferred_element_type=F32)
@@ -136,8 +209,32 @@
             ).astype(BF16)
         return 0
 
+    for direction, present in ((0, has_prev), (1, has_next)):
+
+        @pl.when(present)
+        def _(direction=direction):
+            for i in range(3):
+                edge_copy(i, direction).wait_recv()
+
+    off = 0
+    for i in range(3):
+        n = edges[i].shape[1]
+        low = edges[i][...].astype(F32)
+        high = edges[3 + i][...].astype(F32)
+        halo_ref[0:2, off : off + n] = jnp.where(has_prev, low[EDGE - 2 :], 0.0)
+        halo_ref[2:3, off : off + n] = jnp.where(has_next, high[0:1], 0.0)
+        off += n
     lax.fori_loop(0, pairs, first, 0)
-    pl.semaphore_wait(barrier, greeted)
+    for o in range(1, sp):
+        for i in range(5):
+            param_copy(i, lax.rem(here + o, sp), here).wait_send()
+    for direction, present in ((0, has_next), (1, has_prev)):
+
+        @pl.when(present)
+        def _(direction=direction):
+            for i in range(3):
+                edge_copy(i, direction).wait_send()
+
 
     def inner(p, _):
         x_at = pl.ds(pl.multiple_of(p * x_w, 128), x_w)
@@ -366,38 +463,6 @@
     groups = b.shape[1] // STATE
     heads = ahead.shape[2]
     pairs = groups // 2
-    xw, bw, hw = wx.shape[1], wb.shape[1], offset.shape[1]
-    taps = jnp.concatenate([wx, wb, wc], axis=1).astype(F32)
-    small = jnp.concatenate([offset, fading], axis=0)
-    packed = jnp.concatenate([taps, jnp.pad(small, ((0, 0), (0, taps.shape[1] - hw)))], axis=0)
-    every = lax.all_gather(packed, "sp")
-    whole = jnp.transpose(every, (1, 0, 2))
-    w = jnp.concatenate(
-        [
-            whole[:, :, :xw].reshape(8, -1),
-            whole[:, :, xw : xw + bw].reshape(8, -1),
-            whole[:, :, xw + bw :].reshape(8, -1),
-        ],
-        axis=1,
-    )
-    tail = jnp.zeros((128 - 2 * heads,), F32)
-    flat = whole[4:8, :, :hw].reshape(4, heads)
-    prm = jnp.stack(
-        [jnp.concatenate([flat[0], flat[1], tail]), jnp.concatenate([flat[2], flat[3], tail])]
-    )
-    prm = jnp.pad(prm, ((0, 6), (0, 0)))
-    count = sp * dp
-    place = [(i % sp) * dp + i // sp for i in range(count)]
-    ring = list(zip(place[:-1], place[1:]))
-    edge = jnp.concatenate([x[-2:], b[-2:], c[-2:]], axis=1)
-    head = jnp.concatenate([x[:1], b[:1], c[:1]], axis=1)
-    before = lax.ppermute(edge, ("sp", "dp"), ring)
-    after = lax.ppermute(head, ("sp", "dp"), [(j, i) for i, j in ring])
-    halo = jnp.pad(jnp.concatenate([before, after], axis=0).astype(F32), ((0, 5), (0, 0)))
-    pad = jnp.zeros((blk, 128 - 2 * heads), F32)
-    inc = jnp.concatenate([ahead[0], back[0], pad], axis=1)
-    spikes = jnp.concatenate([spike[0], spike[0], pad], axis=1)
-
     levels, top = levels_of(sp, dp, groups)
     scratch = [
         pltpu.VMEM((blk, x_total), BF16),
@@ -407,7 +472,14 @@
     ]
     scratch += [pltpu.VMEM((128, 128), F32)] * 5
     rows = x_total
+    params = (wx, wb, wc, offset, fading)
+    width = x_total + 2 * b.shape[1]
+    early = [pltpu.VMEM((sp,) + one.shape, one.dtype) for one in params]
+    early += [pltpu.VMEM((8, width), F32), pltpu.VMEM((8, 128), F32), pltpu.VMEM((8, width), F32)]
+    early += [pltpu.VMEM((EDGE, one.shape[1]), BF16) for one in (x, b, c)] * 2
+    early += [pltpu.SemaphoreType.DMA((2, 5, sp)), pltpu.SemaphoreType.DMA((2, 2, 3))]
     scratch += [pltpu.VMEM((2, rows, STATE), BF16), pltpu.VMEM((8, 128), F32)]
+    scratch += early
     widest = 1
     for _, n, _ in levels:
         widest = max(widest, n)
@@ -429,16 +501,16 @@
         pltpu.VMEM((widest, 128, 128), F32),
     ]
     out = pl.pallas_call(
-        functools.partial(kernel, levels, top, (heads, pairs)),
+        functools.partial(kernel, levels, top, (heads, pairs, sp, dp)),
         out_shape=jax.ShapeDtypeStruct((blk, x_total), BF16),
-        in_specs=[pl.BlockSpec(memory_space=pltpu.VMEM)] * 10,
+        in_specs=[pl.BlockSpec(memory_space=pltpu.VMEM)] * 13,
         out_specs=pl.BlockSpec(memory_space=pltpu.VMEM),
         scratch_shapes=scratch,
         compiler_params=pltpu.CompilerParams(
             collective_id=0, has_side_effects=True, vmem_limit_bytes=60 * 2**20
         ),
         name="mixer",
-    )(x, b, c, z, inc, spikes, prm, w, halo, gain.astype(F32)[None])
+    )(x, b, c, z, ahead[0].T, back[0].T, spike[0].T, *params, gain.astype(F32)[None])
     return out[None]
 
 

time: 88.6 us -> 73.2 us (0.83)
  blocking collectives: 7.96 us -> 0 us
  Pallas kernels: 62.2 us -> 69.6 us
  starting transfers between devices: 5.73 us -> 0 us
  local copies, waits for them, and re-layouts: 8.2 us -> 2.75 us
  other arithmetic: 3.61 us -> 0.6 us
    all_gather x1 -> x0, blocking collectives: 7.96 us -> none  [local(): every = lax.all_gather(packed, 'sp')]
    pallas_call x1, Pallas kernels: 62.2 us -> 69.6 us  [local(): pl.pallas_call(functools.partial(kernel, levels, top, (heads, pairs, sp,...]
    ppermute x2 -> x0, starting transfers between devices: 5.73 us -> none  [the longest x1 3.68 us: local(): before = lax.ppermute(edge, ('sp', 'dp'), ring)]
    slice x5 -> x0, local copies, waits for them, and re-layouts: 3.22 us -> none  [the longest x2 1.61 us: local(): edge = jnp.concatenate([x[-2:], b[-2:], c[-2:]], axis=1)]
    unnamed x27 -> x3, local copies, waits for them, and re-layouts: 4.56 us -> 2.75 us
    concatenate x6 -> x0, other arithmetic: 1.55 us -> none  [the longest x1 0.76 us: local(): spikes = jnp.concatenate([spike[0], spike[0], pad], axis=1)]
  transfers between devices with their start and end apart: 2 -> 0, of which waited for: 0 -> 0; matrix products, arithmetic and copies ran while one was open for 6% -> 0% of each run, Pallas kernels for 0% -> 0%
where the time goes in v1:
time: 73.2 us; the launch traced here: 73 us
  Pallas kernels  69.6 us (95%)
  local copies, waits for them, and re-layouts  2.75 us (4%)
    pallas_call x1, Pallas kernels, local(): pl.pallas_call(functools.partial(kernel, levels, top, (heads, pairs, sp,...  69.6 us
    unnamed x3, local copies, waits for them, and re-layouts  2.75 us

profile of v1, /device:TPU:9, one launch (start us, length us, event | category | flops | bytes accessed | tf_op | source)
XLA Modules:
  0.0 73.0 jit_solution(4202533827802540530)
XLA Ops:
  0.0 0.0 copy-start
  0.0 0.7 copy-done
  0.7 0.6 broadcast_in_dim.11
  1.3 69.6 %mixer.1 = bf16[128,3072]{1,0:T(8,128)(2,1)} custom-call(bf16[128,3072]{1,0:T(8,128)(2,1)} %bitcast.16, bf16[128,2048]{1,0:T(8,128)(2,1)} %bitcast.18, bf16[128,2048]{1,0:T(8,128)(2,1)} %bitcast.19, bf16[128,3072]{1,0:T(8,128)(2,1)} %bitcast.17, f32[48,128]{1,0:T(8,128)} %bitcast.21, f32[48,128]{1,0:T(8,128)} %bitcast.22, f32[48,128]{1,0:T(8,128)} %bitcast.23, ...), custom_call_target="tpu_custom_call" | custom-call | tf_op jit(solution)/shard_map/mixer/pallas_call | solution.py:503
  70.9 2.1 %copy.15 = bf16[1,128,3072]{2,1,0:T(8,128)(2,1)} copy(bf16[1,128,3072]{2,1,0:T(8,128)(2,1)} %bitcast.15) | data formatting | bytes 1572864
Async XLA Ops:
  0.0 0.7 copy-start

commit v2 on v1

--- a/solution.py
+++ b/solution.py
@@ -38,25 +38,29 @@
 
 
 def kernel(levels, top, sizes, *refs):
-    heads, pairs, sp, dp = sizes
+    heads, pairs, chunks, sp, dp = sizes
     (x_ref, b_ref, c_ref, z_ref, ahead_ref, back_ref, spike_ref) = refs[:7]
     params = refs[7:12]
     gain_ref, out_ref = refs[12:14]
-    (xc, bc, cc, y_ref, cum_ref, rate_ref, cum_t, rate_t, fac_ref, first_total, first_log) = refs[14:25]
+    (xc, bc, cc, y_ref, cum_ref, rate_ref, cum_t, rate_t, fac_ref) = refs[14:23]
+    refs = refs[:14] + refs[23:]
     got, w_ref, prm_ref, halo_ref, edges, early_sem, edge_sem = (
-        refs[25:30], refs[30], refs[31], refs[32], refs[33:39], refs[39], refs[40]
+        refs[14:19], refs[19], refs[20], refs[21], refs[22:28], refs[28], refs[29]
     )
-    rest = list(refs[41:])
-    up, up_log, down, stage, totals, logs, sems = [], [], [], [], [first_total], [first_log], []
-    for _ in levels:
-        up.append(rest.pop(0))
-        up_log.append(rest.pop(0))
-        down.append(rest.pop(0))
-        stage.append(rest.pop(0))
-        totals.append(rest.pop(0))
-        logs.append(rest.pop(0))
-        sems.append(rest.pop(0))
-    top_in, top_log, top_sem, incoming, decay = rest
+    rest = list(refs[30:])
+    depth = len(levels)
+    logs = [rest.pop(0) for _ in range(depth + 1)]
+    up_log = [rest.pop(0) for _ in range(depth + 1)]
+    decay = [rest.pop(0) for _ in range(depth + 1)]
+    log_sem = [rest.pop(0) for _ in range(depth + 1)]
+    totals, up, down, stage, sems, incoming = ([] for _ in range(6))
+    for _ in range(chunks):
+        totals.append([rest.pop(0) for _ in range(depth + 1)])
+        up.append([rest.pop(0) for _ in range(depth + 1)])
+        down.append([rest.pop(0) for _ in range(depth)])
+        stage.append([rest.pop(0) for _ in range(depth)])
+        sems.append([rest.pop(0) for _ in range(depth + 1)])
+        incoming.append(rest.pop(0))
     blk = x_ref.shape[0]
     per_pair = heads // pairs
     x_w = per_pair * HEAD_DIM
@@ -161,7 +165,7 @@
     cum_t[...] = cum.T
     rate_t[...] = rate.T
     fac_ref[...] = rate * jnp.exp(last - cum)
-    first_log[...] = jnp.broadcast_to(last, (8, 128))
+    logs[0][...] = jnp.broadcast_to(last, (8, 128))
 
     def rolled(ref, p):
         return pltpu.roll(ref[...], lax.rem(128 - p * per_pair, 128), 1)
@@ -180,10 +184,11 @@
         s = m2 * w_ref[0:1, at] + m1 * w_ref[1:2, at] + v * w_ref[2:3, at] + p1 * w_ref[3:4, at]
         return (s / (1.0 + jnp.exp(-s))).astype(BF16)
 
+    share = pairs // chunks
     x_total = x_ref.shape[1]
     b_total = b_ref.shape[1]
 
-    def first(p, _):
+    def first(c, p, _):
         x_at = pl.ds(pl.multiple_of(p * x_w, 128), x_w)
         b_at = pl.ds(pl.multiple_of(p * b_w, 128), b_w)
         xv = conv(x_ref, p * x_w, x_w, 0)
@@ -203,8 +208,8 @@
             )
             u = lax.dot_general(scaled, bv, (((0,), (0,)), ((), ())), preferred_element_type=F32)
             half = x_w // 2
-            rows = pl.ds(pl.multiple_of(p * x_w, 128), x_w)
-            first_total[d, rows, :] = jnp.concatenate(
+            rows = pl.ds(pl.multiple_of((p - c * share) * x_w, 128), x_w)
+            totals[c][0][d, rows, :] = jnp.concatenate(
                 [u[:half, :STATE], u[half:, STATE:]], axis=0
             ).astype(BF16)
         return 0
@@ -224,18 +229,6 @@
         halo_ref[0:2, off : off + n] = jnp.where(has_prev, low[EDGE - 2 :], 0.0)
         halo_ref[2:3, off : off + n] = jnp.where(has_next, high[0:1], 0.0)
         off += n
-    lax.fori_loop(0, pairs, first, 0)
-    for o in range(1, sp):
-        for i in range(5):
-            param_copy(i, lax.rem(here + o, sp), here).wait_send()
-    for direction, present in ((0, has_next), (1, has_prev)):
-
-        @pl.when(present)
-        def _(direction=direction):
-            for i in range(3):
-                edge_copy(i, direction).wait_send()
-
-
     def inner(p, _):
         x_at = pl.ds(pl.multiple_of(p * x_w, 128), x_w)
         b_at = pl.ds(pl.multiple_of(p * b_w, 128), b_w)
@@ -278,150 +271,201 @@
             device_id_type=pl.DeviceIdType.MESH,
         )
 
-    def expand(slot, tile):
-        decay[slot] = jnp.exp(jnp.broadcast_to(tile[0:1, :], (128, 128)).T)
-
-    slots = len(levels) + 1
-    cuts = [(i * pairs) // slots for i in range(slots + 1)]
-    base = jnp.int32(0)
-    bases = []
-    for k, level in enumerate(levels):
-        n = level[1]
-        me = digit_of(level)
-        total, log = totals[k], logs[k]
+    every_level = levels + (top,)
+    head_share = heads // chunks
+    bases = [jnp.int32(0)]
+    size = head_share
+    for level in levels:
+        size = size // level[1]
+        bases.append(bases[-1] + digit_of(level) * size)
+    pending = [[] for _ in range(chunks)]
+
+    def head_rows(h):
+        return pl.ds(pl.multiple_of(h * HEAD_DIM, HEAD_DIM), HEAD_DIM)
+
+    def log_copy(k, member, slot):
+        sem = log_sem[k]
+        return copy(
+            logs[k], up_log[k].at[slot], sem.at[0, member], sem.at[1, slot], every_level[k], member
+        )
+
+    def start_up(c, k):
+        level = every_level[k]
+        n, me = level[1], digit_of(level)
+        total, sem = totals[c][k], sems[c][k]
         rows = total.shape[1] // n
-        sem = sems[k]
-        pending = []
         for o in range(1, n):
             m = lax.rem(me + o, n)
-            part = total.at[:, pl.ds(pl.multiple_of(m * rows, 64), rows), :]
-            pending.append(copy(part, up[k].at[me], sem.at[0, m], sem.at[1, me], level, m))
-            pending.append(copy(log, up_log[k].at[me], sem.at[2, m], sem.at[3, me], level, m))
-        for one in pending:
+            if c == 0:
+                pending[c].append(log_copy(k, m, me))
+            if k < depth:
+                part = total.at[:, pl.ds(pl.multiple_of(m * rows, 64), rows), :]
+            else:
+                part = total.at[jnp.where(m < me, 1, 0)]
+            pending[c].append(
+                copy(part, up[c][k].at[me], sem.at[0, m], sem.at[1, me], level, m)
+            )
+        for one in pending[c]:
             one.start()
-        up[k][me] = total[:, pl.ds(pl.multiple_of(me * rows, 64), rows), :]
-        up_log[k][me] = log[...]
-        lax.fori_loop(cuts[k], cuts[k + 1], inner, 0)
-        for one in pending:
+        if k < depth:
+            up[c][k][me] = total[:, pl.ds(pl.multiple_of(me * rows, 64), rows), :]
+        if c == 0:
+            up_log[k][me] = logs[k][...]
+
+    def flush(c):
+        for one in pending[c]:
             one.wait_send()
+        pending[c].clear()
+
+    def finish_up(c, k):
+        level = every_level[k]
+        n, me = level[1], digit_of(level)
+        total, sem = totals[c][k], sems[c][k]
+        flush(c)
         for o in range(1, n):
             s = lax.rem(me + o, n)
-            part = total.at[:, pl.ds(0, rows), :]
-            copy(part, up[k].at[s], sem.at[0, s], sem.at[1, s], level, s).wait_recv()
-            copy(log, up_log[k].at[s], sem.at[2, s], sem.at[3, s], level, s).wait_recv()
-        base = base + me * (rows // HEAD_DIM)
-        bases.append(base)
-        log_sum = up_log[k][0]
-        for m in range(1, n):
-            log_sum = log_sum + up_log[k][m]
-        logs[k + 1][...] = log_sum
-        for m in range(n):
-            expand(m, up_log[k][m])
-
-        def gather(h, _, k=k, n=n, base=base):
-            at = pl.ds(pl.multiple_of(h * HEAD_DIM, HEAD_DIM), HEAD_DIM)
-            f = up[k][0, 0, at, :].astype(F32)
-            b = up[k][n - 1, 1, at, :].astype(F32)
+            if c == 0:
+                log_copy(k, s, s).wait_recv()
+            part = total.at[:, pl.ds(0, total.shape[1] // n), :] if k < depth else total.at[0]
+            copy(part, up[c][k].at[s], sem.at[0, s], sem.at[1, s], level, s).wait_recv()
+        if c == 0:
+
+            def expand(m, _):
+                decay[k][m] = jnp.exp(jnp.broadcast_to(up_log[k][m][0:1, :], (128, 128)).T)
+                return 0
+
+            lax.fori_loop(0, n, expand, 0)
+            if k < depth:
+                log_sum = up_log[k][0]
+                for m in range(1, n):
+                    log_sum = log_sum + up_log[k][m]
+                logs[k + 1][...] = log_sum
+
+    def gather(c, k):
+        n = levels[k][1]
+        base = c * head_share + bases[k + 1]
+        part, new = up[c][k], totals[c][k + 1]
+
+        def one_head(h, _):
+            at = head_rows(h)
+            f = part[0, 0, at, :].astype(F32)
+            b = part[n - 1, 1, at, :].astype(F32)
             for m in range(1, n):
-                f = f * decay[m, pl.ds(base + h, 1), :] + up[k][m, 0, at, :].astype(F32)
                 r = n - 1 - m
-                b = b * decay[r, pl.ds(heads + base + h, 1), :] + up[k][r, 1, at, :].astype(F32)
-            totals[k + 1][0, at, :] = f.astype(BF16)
-            totals[k + 1][1, at, :] = b.astype(BF16)
+                f = f * decay[k][m, pl.ds(base + h, 1), :] + part[m, 0, at, :].astype(F32)
+                b = b * decay[k][r, pl.ds(heads + base + h, 1), :] + part[r, 1, at, :].astype(F32)
+            new[0, at, :] = f.astype(BF16)
+            new[1, at, :] = b.astype(BF16)
             return 0
 
-        lax.fori_loop(0, rows // HEAD_DIM, gather, 0)
-
-    n = top[1]
-    me = digit_of(top)
-    total, log = totals[-1], logs[-1]
-    pending = []
-    for o in range(1, n):
-        m = lax.rem(me + o, n)
-        d = jnp.where(m < me, 1, 0)
-        pending.append(
-            copy(total.at[d], top_in.at[me], top_sem.at[0, m], top_sem.at[1, me], top, m)
-        )
-        pending.append(copy(log, top_log.at[me], top_sem.at[2, m], top_sem.at[3, me], top, m))
-    for one in pending:
-        one.start()
-    lax.fori_loop(cuts[-2], cuts[-1], inner, 0)
-    for one in pending:
-        one.wait_send()
-    for o in range(1, n):
-        s = lax.rem(me + o, n)
-        copy(total.at[0], top_in.at[s], top_sem.at[0, s], top_sem.at[1, s], top, s).wait_recv()
-        copy(log, top_log.at[s], top_sem.at[2, s], top_sem.at[3, s], top, s).wait_recv()
-    incoming[...] = jnp.zeros_like(incoming)
-
-    def carry(s, d):
-        expand(0, top_log[s])
-
-        def one_head(h, _):
-            at = pl.ds(pl.multiple_of(h * HEAD_DIM, HEAD_DIM), HEAD_DIM)
-            factor = decay[0, pl.ds(d * heads + base + h, 1), :]
-            incoming[d, at, :] = incoming[d, at, :] * factor + top_in[s, at, :].astype(F32)
+        lax.fori_loop(0, new.shape[1] // HEAD_DIM, one_head, 0)
+
+    def enter(c):
+        n, me = top[1], digit_of(top)
+        base = c * head_share + bases[-1]
+        into = incoming[c]
+        into[...] = jnp.zeros_like(into)
+
+        def carry(s, d):
+            def one_head(h, _):
+                at = head_rows(h)
+                factor = decay[depth][s, pl.ds(d * heads + base + h, 1), :]
+                into[d, at, :] = into[d, at, :] * factor + up[c][depth][s, at, :].astype(F32)
+                return 0
+
+            lax.fori_loop(0, into.shape[1] // HEAD_DIM, one_head, 0)
             return 0
 
-        lax.fori_loop(0, total.shape[1] // HEAD_DIM, one_head, 0)
-        return 0
-
-    lax.fori_loop(0, me, lambda s, _: carry(s, 0), 0)
-    lax.fori_loop(0, n - 1 - me, lambda i, _: carry(n - 1 - i, 1), 0)
-
-    for k in reversed(range(len(levels))):
+        lax.fori_loop(0, me, lambda s, _: carry(s, 0), 0)
+        lax.fori_loop(0, n - 1 - me, lambda i, _: carry(n - 1 - i, 1), 0)
+
+    def start_down(c, k):
         level = levels[k]
-        n = level[1]
-        me = digit_of(level)
-        sem = sems[k]
-        rows = totals[k].shape[1] // n
-        source = incoming if k == len(levels) - 1 else down[k + 1]
-        for m in range(n):
-            expand(m, up_log[k][m])
-
-        def spread(h, _, k=k, n=n, base=bases[k], source=source):
-            at = pl.ds(pl.multiple_of(h * HEAD_DIM, HEAD_DIM), HEAD_DIM)
+        n, me = level[1], digit_of(level)
+        sem = sems[c][k]
+        rows = totals[c][k].shape[1] // n
+        base = c * head_share + bases[k + 1]
+        source = incoming[c] if k == depth - 1 else down[c][k + 1]
+        part, out = up[c][k], stage[c][k]
+
+        def spread(h, _):
+            at = head_rows(h)
             f = source[0, at, :].astype(F32)
             b = source[1, at, :].astype(F32)
             for m in range(n):
                 r = n - 1 - m
-                stage[k][m, 0, at, :] = f.astype(BF16)
-                stage[k][r, 1, at, :] = b.astype(BF16)
+                out[m, 0, at, :] = f.astype(BF16)
+                out[r, 1, at, :] = b.astype(BF16)
                 if m < n - 1:
-                    f = f * decay[m, pl.ds(base + h, 1), :] + up[k][m, 0, at, :].astype(F32)
-                    b = b * decay[r, pl.ds(heads + base + h, 1), :] + up[k][r, 1, at, :].astype(F32)
+                    f = f * decay[k][m, pl.ds(base + h, 1), :] + part[m, 0, at, :].astype(F32)
+                    down_factor = decay[k][r, pl.ds(heads + base + h, 1), :]
+                    b = b * down_factor + part[r, 1, at, :].astype(F32)
             return 0
 
         lax.fori_loop(0, rows // HEAD_DIM, spread, 0)
         mine = pl.ds(pl.multiple_of(me * rows, 64), rows)
-        pending = []
         for o in range(1, n):
             m = lax.rem(me + o, n)
-            pending.append(
-                copy(stage[k].at[m], down[k].at[:, mine, :], sem.at[4, m], sem.at[5, me], level, m)
+            pending[c].append(
+                copy(out.at[m], down[c][k].at[:, mine, :], sem.at[2, m], sem.at[3, me], level, m)
             )
-        for one in pending:
+        for one in pending[c]:
             one.start()
-        down[k][:, mine, :] = stage[k][me]
-        for one in pending:
-            one.wait_send()
+        down[c][k][:, mine, :] = out[me]
+
+    def finish_down(c, k):
+        level = levels[k]
+        n, me = level[1], digit_of(level)
+        sem = sems[c][k]
+        rows = totals[c][k].shape[1] // n
+        flush(c)
         for o in range(1, n):
             s = lax.rem(me + o, n)
             theirs = pl.ds(pl.multiple_of(s * rows, 64), rows)
             copy(
-                stage[k].at[s], down[k].at[:, theirs, :], sem.at[4, s], sem.at[5, s], level, s
+                stage[c][k].at[s], down[c][k].at[:, theirs, :], sem.at[2, s], sem.at[3, s], level, s
             ).wait_recv()
 
-    final = down[0] if levels else incoming
+    for c in range(chunks):
+        lax.fori_loop(c * share, (c + 1) * share, functools.partial(first, c), 0)
+        start_up(c, 0)
+    for o in range(1, sp):
+        for i in range(5):
+            param_copy(i, lax.rem(here + o, sp), here).wait_send()
+    for direction, present in ((0, has_next), (1, has_prev)):
+
+        @pl.when(present)
+        def _(direction=direction):
+            for i in range(3):
+                edge_copy(i, direction).wait_send()
+
+
+    gaps = chunks * depth
+    cuts = [(i * pairs) // gaps for i in range(gaps + 1)]
+    for k in range(depth):
+        for c in range(chunks):
+            finish_up(c, k)
+            gather(c, k)
+            start_up(c, k + 1)
+            at = k * chunks + c
+            lax.fori_loop(cuts[at], cuts[at + 1], inner, 0)
+    for c in range(chunks):
+        finish_up(c, depth)
+        enter(c)
+        start_down(c, depth - 1)
+    for k in reversed(range(1, depth)):
+        for c in range(chunks):
+            finish_down(c, k)
+            start_down(c, k - 1)
+
     cum_ref[...] = jnp.exp(cum_ref[...])
 
-    def last_part(p, _):
-        x_at = pl.ds(pl.multiple_of(p * x_w, 128), x_w)
+    def last_part(c, p, _):
         cv = cc[:, pl.ds(pl.multiple_of(p * b_w, 128), b_w)]
         cols = rolled(cum_ref, p)
         carried = []
         for d in range(2):
-            st = final[d, x_at, :].astype(BF16)
+            st = down[c][0][d, pl.ds(pl.multiple_of((p - c * share) * x_w, 128), x_w), :]
             got = [
                 lax.dot_general(
                     cv[:, g * STATE : (g + 1) * STATE],
@@ -454,7 +498,9 @@
             out_ref[:, at] = (gated * lax.rsqrt(mean + 1e-6) * gain_ref[0:1, at]).astype(BF16)
         return 0
 
-    lax.fori_loop(0, pairs, last_part, 0)
+    for c in range(chunks):
+        finish_down(c, 0)
+        lax.fori_loop(c * share, (c + 1) * share, functools.partial(last_part, c), 0)
 
 
 def local(sp, dp, x, b, c, z, ahead, back, spike, wx, wb, wc, offset, fading, gain):
@@ -471,37 +517,36 @@
         pltpu.VMEM((blk, x_total), F32),
     ]
     scratch += [pltpu.VMEM((128, 128), F32)] * 5
-    rows = x_total
     params = (wx, wb, wc, offset, fading)
     width = x_total + 2 * b.shape[1]
     early = [pltpu.VMEM((sp,) + one.shape, one.dtype) for one in params]
     early += [pltpu.VMEM((8, width), F32), pltpu.VMEM((8, 128), F32), pltpu.VMEM((8, width), F32)]
     early += [pltpu.VMEM((EDGE, one.shape[1]), BF16) for one in (x, b, c)] * 2
     early += [pltpu.SemaphoreType.DMA((2, 5, sp)), pltpu.SemaphoreType.DMA((2, 2, 3))]
-    scratch += [pltpu.VMEM((2, rows, STATE), BF16), pltpu.VMEM((8, 128), F32)]
     scratch += early
-    widest = 1
-    for _, n, _ in levels:
-        widest = max(widest, n)
-        scratch += [
-            pltpu.VMEM((n, 2, rows // n, STATE), BF16),
-            pltpu.VMEM((n, 8, 128), F32),
-            pltpu.VMEM((2, rows, STATE), BF16),
-            pltpu.VMEM((n, 2, rows // n, STATE), BF16),
-            pltpu.VMEM((2, rows // n, STATE), BF16),
-            pltpu.VMEM((8, 128), F32),
-            pltpu.SemaphoreType.DMA((6, n)),
-        ]
-        rows //= n
-    scratch += [
-        pltpu.VMEM((top[1], rows, STATE), BF16),
-        pltpu.VMEM((top[1], 8, 128), F32),
-        pltpu.SemaphoreType.DMA((4, top[1])),
-        pltpu.VMEM((2, rows, STATE), F32),
-        pltpu.VMEM((widest, 128, 128), F32),
-    ]
+    split = 1
+    for level in levels:
+        split *= level[1]
+    chunks = 2 if groups % (2 * split) == 0 else 1
+    counts = [level[1] for level in levels] + [top[1]]
+    scratch += [pltpu.VMEM((8, 128), F32)] * len(counts)
+    scratch += [pltpu.VMEM((n, 8, 128), F32) for n in counts]
+    scratch += [pltpu.VMEM((n, 128, 128), F32) for n in counts]
+    scratch += [pltpu.SemaphoreType.DMA((2, n)) for n in counts]
+    for _ in range(chunks):
+        held = [x_total // chunks]
+        for n in counts[:-1]:
+            held.append(held[-1] // n)
+        slabs = list(zip(counts[:-1], held[1:]))
+        scratch += [pltpu.VMEM((2, rows, STATE), BF16) for rows in held]
+        scratch += [pltpu.VMEM((n, 2, rows, STATE), BF16) for n, rows in slabs]
+        scratch += [pltpu.VMEM((counts[-1], held[-1], STATE), BF16)]
+        scratch += [pltpu.VMEM((2, rows, STATE), BF16) for rows in held[:-1]]
+        scratch += [pltpu.VMEM((n, 2, rows, STATE), BF16) for n, rows in slabs]
+        scratch += [pltpu.SemaphoreType.DMA((4, n)) for n in counts]
+        scratch += [pltpu.VMEM((2, held[-1], STATE), F32)]
     out = pl.pallas_call(
-        functools.partial(kernel, levels, top, (heads, pairs, sp, dp)),
+        functools.partial(kernel, levels, top, (heads, pairs, chunks, sp, dp)),
         out_shape=jax.ShapeDtypeStruct((blk, x_total), BF16),
         in_specs=[pl.BlockSpec(memory_space=pltpu.VMEM)] * 13,
         out_specs=pl.BlockSpec(memory_space=pltpu.VMEM),

time: 73.2 us -> 62.1 us (0.85)
  Pallas kernels: 69.6 us -> 57.8 us
    pallas_call x1, Pallas kernels: 69.6 us -> 57.8 us  [local(): pl.pallas_call(functools.partial(kernel, levels, top, (heads, pairs, chun...]
where the time goes in v2:
time: 62.1 us; the launch traced here: 61.2 us
  Pallas kernels  57.8 us (93%)
  local copies, waits for them, and re-layouts  2.75 us (4%)
    pallas_call x1, Pallas kernels, local(): pl.pallas_call(functools.partial(kernel, levels, top, (heads, pairs, chun...  57.8 us
    unnamed x3, local copies, waits for them, and re-layouts  2.75 us

profile of v2, /device:TPU:9, one launch (start us, length us, event | category | flops | bytes accessed | tf_op | source)
XLA Modules:
  0.0 61.2 jit_solution(17215395492030648556)
XLA Ops:
  0.0 0.0 copy-start
  0.0 0.7 %copy-done = bf16[3072]{0:T(1024)(128)(2,1)S(1)} copy-done((bf16[3072]{0:T(1024)(128)(2,1)S(1)}, bf16[3072]{0:T(1024)(128)(2,1)}, u32[]{:S(2)}) %copy-start) | copy-done | bytes 6168
  0.7 0.6 broadcast_in_dim.11
  1.3 57.8 %mixer.1 = bf16[128,3072]{1,0:T(8,128)(2,1)} custom-call(bf16[128,3072]{1,0:T(8,128)(2,1)} %bitcast.16, bf16[128,2048]{1,0:T(8,128)(2,1)} %bitcast.18, bf16[128,2048]{1,0:T(8,128)(2,1)} %bitcast.19, bf16[128,3072]{1,0:T(8,128)(2,1)} %bitcast.17, f32[48,128]{1,0:T(8,128)} %bitcast.21, f32[48,128]{1,0:T(8,128)} %bitcast.22, f32[48,128]{1,0:T(8,128)} %bitcast.23, ...), custom_call_target="tpu_custom_call" | custom-call | tf_op jit(solution)/shard_map/mixer/pallas_call | solution.py:548
  59.1 2.1 %copy.15 = bf16[1,128,3072]{2,1,0:T(8,128)(2,1)} copy(bf16[1,128,3072]{2,1,0:T(8,128)(2,1)} %bitcast.15) | data formatting | bytes 1572864
Async XLA Ops:
  0.0 0.7 %copy-start = (bf16[3072]{0:T(1024)(128)(2,1)S(1)}, bf16[3072]{0:T(1024)(128)(2,1)}, u32[]{:S(2)}) copy-start(bf16[3072]{0:T(1024)(128)(2,1)} %param.25) | copy-start | bytes 18436
